TPU v7x, 256 devices: a whole 4x4x8 slice. The times are simulated.
256 devices in a mesh: ep: 16 (over y, x), tp: 16 (over z, core).
Axes of the slice: x: 4, y: 4, z: 8, core: 2. Of those that a mesh axis runs over, the one named last changes fastest.
Arguments:
- layer_in: bfloat16 [512, 2048], P('ep'), may hold values from -6 to 6
- attn_gain: float32 [2048], replicated, may hold values from 0.1 to 1.9
- query_weight: bfloat16 [2048, 1024], P(None, 'tp'), may hold values from -0.125 to 0.125
- key_weight: bfloat16 [2048, 1024], P(None, 'tp'), may hold values from -0.125 to 0.125
- value_weight: bfloat16 [2048, 1024], P(None, 'tp'), may hold values from -0.125 to 0.125
- forget_weight: bfloat16 [2048, 16], replicated, may hold values from -0.125 to 0.125
- forget_bias: float32 [16], replicated, may hold values from -2 to 3
- out_weight: bfloat16 [1024, 2048], P('tp'), may hold values from -0.1875 to 0.1875
- kv_cache: bfloat16 [512, 16, 1024, 128], P('ep', 'tp'), may hold values from -110 to 110
- cum_gates: float32 [512, 16, 1024], P('ep', 'tp'), may hold values from -144 to 0, as said below
- lengths: int32 [512], P('ep'), may hold values from 512 to 1024, as said below
- ffn_gain: float32 [2048], replicated, may hold values from 0.1 to 1.9
- route_ids: int32 [512, 6], P('ep'), may hold values from 0 to 127, all different within a row; in each aligned block of 32 rows (0 to 31, 32 to 63, ...) at most 2 rows name the same one
- route_weights: float32 [512, 6], P('ep'), may hold values from 0.1 to 1
- shared_gate: bfloat16 [2048, 512], P(None, 'tp'), may hold values from -0.125 to 0.125
- shared_up: bfloat16 [2048, 512], P(None, 'tp'), may hold values from -0.125 to 0.125
- shared_down: bfloat16 [512, 2048], P('tp'), may hold values from -0.25 to 0.25
- expert_gate: bfloat16 [256, 2048, 256], P(('ep', 'tp')), may hold values from -0.125 to 0.125
- expert_up: bfloat16 [256, 2048, 256], P(('ep', 'tp')), may hold values from -0.125 to 0.125
- expert_down: bfloat16 [256, 256, 2048], P(('ep', 'tp')), may hold values from -0.25 to 0.25
Outputs:
- layer_out: bfloat16 [512, 2048], P('ep')
- new_kv: bfloat16 [512, 16, 128], P('ep', 'tp')
Inputs may be any that keep to these rules, and one draw needn't show every extreme that they name: `cum_gates`: never rising along positions. `lengths`: every length is at most 1024, and some sequence's length is exactly 1024. `route_ids`: each row names 6 different experts. Among the 32 rows of one index of ep (aligned blocks), no expert is named by more than 2 rows, and in some block one expert is named by exactly 2 rows.
All inputs are finite; a program needn't handle non-finite values.
Results may differ from a plain program's by a relative error of at most 0.019.
Values may be sent and summed in bfloat16 or wider, within the bound.
No kernel may reach another device: no remote copies, remote signals or barrier semaphores. Data moves between devices by JAX's collectives and lax.ppermute only.
A program may use at most 64 MiB of HBM per device.

v0:
```python
import jax
import jax.numpy as jnp
from jax import lax
from jax.sharding import PartitionSpec as P

NORM_EPS = 1e-06


def cut_along(shard, dim, peers):
    before, after = (shard.shape[:dim], shard.shape[dim + 1 :])
    return jnp.moveaxis(shard.reshape(*before, peers, -1, *after), dim, 0)


def summed_on_arrival(shard, axis, dim):
    tiles = cut_along(shard, dim, lax.axis_size(axis))
    arrived = lax.all_to_all(tiles, axis, split_axis=0, concat_axis=0, tiled=True)
    return arrived.astype(jnp.float32).sum(axis=0)


def in_one_piece(arrays, axis, dim, along):
    both = jnp.concatenate(arrays, axis=along)
    filled, at, outs = (lax.all_gather(both, axis, axis=dim, tiled=True), 0, [])
    for a in arrays:
        outs.append(lax.slice_in_dim(filled, at, at + a.shape[along], axis=along))
        at += a.shape[along]
    return tuple(outs)


def rms_scale(stream, gain):
    wide = stream.astype(jnp.float32)
    factor = lax.rsqrt(jnp.mean(wide * wide, axis=-1, keepdims=True) + NORM_EPS)
    return (wide * factor * gain).astype(jnp.bfloat16)


def project(normed, weight):
    return jnp.dot(normed, weight, preferred_element_type=jnp.float32).astype(jnp.bfloat16)


def attend(queries, new_key, new_value, forget, kv_block, cum_block, length_block):
    head_size = queries.shape[-1]
    cache_span = kv_block.shape[2]
    positions = jnp.arange(cache_span, dtype=jnp.int32)
    inside = positions[None, None, :] < length_block[:, None, None]
    at_last = positions[None, None, :] == (length_block - 1)[:, None, None]
    latest = jnp.sum(jnp.where(at_last, cum_block, 0.0), axis=-1)
    scaling = head_size ** (-0.5)
    cached_keys = kv_block[..., :head_size]
    cached_values = kv_block[..., head_size:]
    scores = (
        jnp.einsum("shd,shld->shl", queries, cached_keys, preferred_element_type=jnp.float32)
        * scaling
    )
    scores = jnp.where(inside, scores + (latest + forget)[..., None] - cum_block, -jnp.inf)
    itself = jnp.sum(queries.astype(jnp.float32) * new_key.astype(jnp.float32), axis=-1) * scaling
    highest = jnp.maximum(jnp.max(scores, axis=-1), itself)
    earlier = jnp.exp(scores - highest[..., None])
    own_term = jnp.exp(itself - highest)
    denominator = jnp.sum(earlier, axis=-1) + own_term
    past_probs = (earlier / denominator[..., None]).astype(jnp.bfloat16)
    own_probs = (own_term / denominator).astype(jnp.bfloat16)
    blended = jnp.einsum(
        "shl,shld->shd", past_probs, cached_values, preferred_element_type=jnp.float32
    )
    blended = blended + own_probs.astype(jnp.float32)[..., None] * new_value.astype(jnp.float32)
    return blended.astype(jnp.bfloat16)


def body(
    layer_in,
    attn_gain,
    query_weight,
    key_weight,
    value_weight,
    forget_weight,
    forget_bias,
    out_weight,
    kv_cache,
    cum_gates,
    lengths,
    ffn_gain,
    route_ids,
    route_weights,
    shared_gate,
    shared_up,
    shared_down,
    expert_gate,
    expert_up,
    expert_down,
):
    row_count = layer_in.shape[0]
    width = layer_in.shape[1]
    heads_here = kv_cache.shape[1]
    head_size = kv_cache.shape[3] // 2
    normed = rms_scale(layer_in, attn_gain)
    queries = project(normed, query_weight).reshape(row_count, heads_here, head_size)
    new_key = project(normed, key_weight).reshape(row_count, heads_here, head_size)
    new_value = project(normed, value_weight).reshape(row_count, heads_here, head_size)
    new_kv = jnp.concatenate([new_key, new_value], axis=-1)
    first_head = lax.axis_index("tp") * heads_here
    gate_logits = jnp.dot(normed, forget_weight, preferred_element_type=jnp.float32) + forget_bias
    forget = jax.nn.log_sigmoid(lax.dynamic_slice_in_dim(gate_logits, first_head, heads_here, 1))
    attended = attend(queries, new_key, new_value, forget, kv_cache, cum_gates, lengths)
    head_part = jnp.dot(
        attended.reshape(row_count, heads_here * head_size),
        out_weight,
        preferred_element_type=jnp.float32,
    )
    slice_rows = row_count // lax.axis_size("tp")
    slice_start = lax.axis_index("tp") * slice_rows
    head_slice = summed_on_arrival(head_part.astype(jnp.bfloat16), "tp", 0)
    own_stream = lax.dynamic_slice_in_dim(layer_in, slice_start, slice_rows, 0)
    middle_slice = (own_stream.astype(jnp.float32) + head_slice).astype(jnp.bfloat16)
    hidden_slice = rms_scale(middle_slice, ffn_gain)
    middle, hidden_in = in_one_piece((middle_slice, hidden_slice), "tp", 0, 1)
    shared_hidden = (
        jax.nn.silu(jnp.dot(hidden_in, shared_gate, preferred_element_type=jnp.float32))
        * jnp.dot(hidden_in, shared_up, preferred_element_type=jnp.float32)
    ).astype(jnp.bfloat16)
    shared_part = jnp.dot(shared_hidden, shared_down, preferred_element_type=jnp.float32)
    my_gate = expert_gate[0]
    my_up = expert_up[0]
    my_down = expert_down[0]
    ep_count = lax.axis_size("ep")
    pair_count = lax.axis_size("tp") // 2
    column = lax.axis_index("tp") // 2
    picks = route_ids.shape[1]
    experts = ep_count * pair_count
    capacity = max(2, 4 * row_count * picks // (3 * experts))
    targets = jnp.arange(ep_count, dtype=jnp.int32) * pair_count + column
    matches = route_ids[:, :, None] == targets[None, None, :]
    member = jnp.any(matches, axis=1).astype(jnp.int32)
    weight = jnp.sum(jnp.where(matches, route_weights[:, :, None], 0.0), axis=1)
    ranking = jnp.cumsum(member, axis=0) - member
    slot_numbers = jnp.arange(capacity, dtype=jnp.int32)
    placement = (member[:, :, None] == 1) & (ranking[:, :, None] == slot_numbers[None, None, :])
    dispatch = jnp.einsum(
        "rs,rd->sd",
        placement.reshape(row_count, ep_count * capacity).astype(jnp.bfloat16),
        hidden_in,
        preferred_element_type=jnp.float32,
    ).astype(jnp.bfloat16)
    dispatch = dispatch.reshape(ep_count, capacity, width)
    received = lax.all_to_all(dispatch, "ep", split_axis=0, concat_axis=0, tiled=True)
    count = received.shape[1]
    batch_rows = received.reshape(ep_count * count, width)
    hidden = (
        jax.nn.silu(jnp.dot(batch_rows, my_gate, preferred_element_type=jnp.float32))
        * jnp.dot(batch_rows, my_up, preferred_element_type=jnp.float32)
    ).astype(jnp.bfloat16)
    served = jnp.dot(hidden, my_down, preferred_element_type=jnp.float32).reshape(
        ep_count, count, width
    )
    returned = lax.all_to_all(
        served.astype(jnp.bfloat16), "ep", split_axis=0, concat_axis=0, tiled=True
    ).astype(served.dtype)
    shares = (placement.astype(jnp.float32) * weight[:, :, None]).reshape(
        row_count, ep_count * capacity
    )
    routed = jnp.dot(
        shares,
        returned.reshape(ep_count * capacity, width),
        precision=lax.Precision.HIGHEST,
        preferred_element_type=jnp.float32,
    )
    mixed_slice = summed_on_arrival((shared_part + routed).astype(jnp.bfloat16), "tp", 0)
    own_middle = lax.dynamic_slice_in_dim(middle, slice_start, slice_rows, 0)
    out_slice = (own_middle.astype(jnp.float32) + mixed_slice).astype(jnp.bfloat16)
    layer_out = lax.all_gather(out_slice, "tp", axis=0, tiled=True)
    return (layer_out, new_kv)


def solution(mesh):
    placed = (
        P("ep", None),
        P(),
        P(None, "tp"),
        P(None, "tp"),
        P(None, "tp"),
        P(),
        P(),
        P("tp", None),
        P("ep", "tp", None, None),
        P("ep", "tp", None),
        P("ep"),
        P(),
        P("ep", None),
        P("ep", None),
        P(None, "tp"),
        P(None, "tp"),
        P("tp", None),
        P(("ep", "tp"), None, None),
        P(("ep", "tp"), None, None),
        P(("ep", "tp"), None, None),
    )
    return jax.shard_map(
        body,
        mesh=mesh,
        in_specs=placed,
        out_specs=(P("ep", None), P("ep", "tp", None)),
        check_vma=False,
    )
```

profile of v0, /device:TPU:1, one launch (start us, length us, event | category | flops | bytes accessed | tf_op | source)
XLA Modules:
  0.0 121.0 jit_solution(8280109137043809349)
XLA Ops:
  0.7 1.1 fusion.13
  2.5 1.1 fusion.55
  3.7 1.3 %convolution_convert_fusion.5 = bf16[32,64]{1,0:T(8,128)(2,1)S(1)} fusion(bf16[2048,64]{0,1:T(8,128)(2,1)} %param.22, bf16[32,2048]{1,0:T(8,128)(2,1)} %param.20, f32[2048]{0:T(1024)} %param.21, f32[32]{0:T(128)S(1)} %add_rsqrt_fusion.1), kind=kOutput, calls=%fused_computation.18 | convolution fusion | flops 8652800 | bytes 405632 | tf_op jit(solution)/shard_map/dot_general | solution.py:36
  5.0 1.4 %dynamic-slice = f32[1]{0:T(128)} dynamic-slice(f32[16]{0:T(128)} %param.26, s32[]{:T(128)S(6)} %select_n.30), dynamic_slice_sizes={1} | dynamic-slice | bytes 12 | tf_op jit(solution)/shard_map/dynamic_slice | solution.py:101
  6.4 1.8 %fusion.21 = f32[32]{0:T(128)S(1)} fusion(f32[32,1,1024]{2,1,0:T(1,128)} %param.29, s32[32]{0:T(128)S(1)} %broadcast_add_fusion), kind=kLoop, calls=%fused_computation.39 | loop fusion | flops 98272 | bytes 131328 | tf_op jit(solution)/shard_map/reduce_sum | solution.py:45
  8.1 5.6 %fusion.2 = f32[32,1,1024]{2,1,0:T(1,128)S(1)} fusion(bf16[32,1,1024,128]{3,2,1,0:T(8,128)(2,1)} %param.28, bf16[32,64,1]{1,0,2:T(8,128)(2,1)S(1)} %bitcast.54), kind=kOutput, calls=%fused_computation.2 | convolution fusion | flops 4194304 | bytes 8523776 | tf_op jit(solution)/shard_map/shd,shld->shl/dot_general | solution.py:50
  15.2 1.0 multiply_reduce_fusion
  16.8 2.6 %fusion = f32[32,1,64]{2,1,0:T(1,128)S(1)} fusion(bf16[32,1,1024,128]{3,2,1,0:T(8,128)(2,1)S(1)} %copy-done.1, f32[32]{0:T(128)S(1)} %get-tuple-element.9, f32[32,1,1024]{2,1,0:T(1,128)S(1)} %get-tuple-element.5, f32[32]{0:T(128)S(1)} %multiply_maximum_fusion), kind=kOutput, calls=%fused_computation | convolution fusion | flops 4292608 | bytes 8528128 | tf_op jit(solution)/shard_map/shl,shld->shd/dot_general | solution.py:61
  20.7 10.0 %all-to-all-start = ((bf16[16,2,2048]{2,1,0:T(2,128)(2,1)}), bf16[16,2,2048]{2,1,0:T(2,128)(2,1)S(1)}, u32[]{:S(2)}, u32[]{:S(2)}) async-start(bf16[16,2,2048]{2,1,0:T(2,128)(2,1)} %reshape.219), calls=%async_computation | async-start | bytes 262144 | tf_op jit(solution)/shard_map/all_to_all | solution.py:16
  33.1 6.5 %all-to-all-done = bf16[16,2,2048]{2,1,0:T(2,128)(2,1)S(1)} async-done(((bf16[16,2,2048]{2,1,0:T(2,128)(2,1)}), bf16[16,2,2048]{2,1,0:T(2,128)(2,1)S(1)}, u32[]{:S(2)}, u32[]{:S(2)}) %all-to-all-start) | async-done | bytes 131104 | tf_op jit(solution)/shard_map/all_to_all | solution.py:16
  39.9 16.6 %all-gather = bf16[16,2,4096]{2,1,0:T(2,128)(2,1)} all-gather(bf16[1,2,4096]{2,1,0:T(2,128)(2,1)S(1)} %maximum_bitcast_fusion), channel_id=1, replica_groups=mesh['ep'=16,'tp'=16] {'tp'}, dimensions={0}, use_global_device_ids=true | all-gather | bytes 278528 | tf_op jit(solution)/shard_map/all_gather | solution.py:22
  56.5 1.0 reshape.226
  59.2 6.8 %all-to-all-start.1 = ((bf16[16,2,2048]{2,1,0:T(2,128)(2,1)}), bf16[16,2,2048]{2,1,0:T(2,128)(2,1)}, u32[]{:S(2)}, u32[]{:S(2)}) async-start(bf16[16,2,2048]{2,1,0:T(2,128)(2,1)} %reshape.220), calls=%async_computation.1 | async-start | bytes 262144 | tf_op jit(solution)/shard_map/all_to_all | solution.py:143
  66.0 1.3 %and_select_fusion = f32[32,16,2]{0,2,1:T(2,128)} fusion(pred[32,16]{0,1:T(8,128)(4,1)} %copy-done.7, f32[32,16]{0,1:T(8,128)} %fusion.28, s32[32,16]{0,1:T(8,128)S(1)} %copy.41), kind=kLoop, calls=%fused_computation.48 | loop fusion | flops 3072 | bytes 8704 | tf_op jit(solution)/shard_map/mul | solution.py:156
  67.4 5.6 %all-to-all-done.1 = bf16[16,2,2048]{2,1,0:T(2,128)(2,1)} async-done(((bf16[16,2,2048]{2,1,0:T(2,128)(2,1)}), bf16[16,2,2048]{2,1,0:T(2,128)(2,1)}, u32[]{:S(2)}, u32[]{:S(2)}) %all-to-all-start.1) | async-done | bytes 131104 | tf_op jit(solution)/shard_map/all_to_all | solution.py:143
  75.6 3.5 %all-to-all-start.2 = ((bf16[16,2,2048]{2,1,0:T(2,128)(2,1)}), bf16[16,2,2048]{2,1,0:T(2,128)(2,1)S(1)}, u32[]{:S(2)}, u32[]{:S(2)}) async-start(bf16[16,2,2048]{2,1,0:T(2,128)(2,1)} %copy.43), calls=%async_computation.2 | async-start | bytes 262144 | tf_op jit(solution)/shard_map/all_to_all | solution.py:153
  79.1 1.1 fusion.25
  80.2 5.7 %all-to-all-done.2 = bf16[16,2,2048]{2,1,0:T(2,128)(2,1)S(1)} async-done(((bf16[16,2,2048]{2,1,0:T(2,128)(2,1)}), bf16[16,2,2048]{2,1,0:T(2,128)(2,1)S(1)}, u32[]{:S(2)}, u32[]{:S(2)}) %all-to-all-start.2) | async-done | bytes 131104 | tf_op jit(solution)/shard_map/all_to_all | solution.py:153
  85.9 1.0 convolution_bitcast_fusion
  87.0 1.3 %fusion.6 = bf16[32,2048]{1,0:T(8,128)(2,1)S(1)} fusion(f32[32,2048]{1,0:T(8,128)S(1)} %convolution_bitcast_fusion, bf16[32,2048]{1,0:T(8,128)(2,1)} %param.36, bf16[2048,32]{0,1:T(8,128)(2,1)} %param.35, bf16[32,4096]{1,0:T(8,128)(2,1)S(1)} %reshape.226, f32[32,32]{1,0:T(8,128)S(1)} %fusion.25), kind=kOutput, calls=%fused_computation.8 | convolution fusion | flops 8525824 | bytes 802816 | tf_op jit(solution)/shard_map/dot_general | solution.py:119
  89.1 7.4 %all-to-all-start.3 = ((bf16[16,2,2048]{2,1,0:T(2,128)(2,1)}), bf16[16,2,2048]{2,1,0:T(2,128)(2,1)S(1)}, u32[]{:S(2)}, u32[]{:S(2)}) async-start(bf16[16,2,2048]{2,1,0:T(2,128)(2,1)} %reshape.222), calls=%async_computation.3 | async-start | bytes 262144 | tf_op jit(solution)/shard_map/all_to_all | solution.py:16
  96.5 1.4 %pad_maximum_fusion = bf16[32,1,128]{2,0,1:T(8,128)(2,1)} fusion(bf16[32,1,64]{2,0,1:T(8,128)(2,1)S(1)} %bitcast.55, bf16[32,1,64]{2,0,1:T(8,128)(2,1)} %bitcast.57), kind=kLoop, calls=%fused_computation.72 | loop fusion | flops 16384 | bytes 16384 | tf_op jit(solution)/shard_map/concatenate | solution.py:98
  97.9 7.5 %all-to-all-done.3 = bf16[16,2,2048]{2,1,0:T(2,128)(2,1)S(1)} async-done(((bf16[16,2,2048]{2,1,0:T(2,128)(2,1)}), bf16[16,2,2048]{2,1,0:T(2,128)(2,1)S(1)}, u32[]{:S(2)}, u32[]{:S(2)}) %all-to-all-start.3) | async-done | bytes 131104 | tf_op jit(solution)/shard_map/all_to_all | solution.py:16
  105.5 14.8 %all-gather.1 = bf16[16,2,2048]{2,1,0:T(2,128)(2,1)S(1)} all-gather(bf16[1,2,2048]{2,1,0:T(2,128)(2,1)S(1)} %fusion.42), channel_id=1, replica_groups=mesh['ep'=16,'tp'=16] {'tp'}, dimensions={0}, use_global_device_ids=true | all-gather | bytes 139264 | tf_op jit(solution)/shard_map/all_gather | solution.py:168
  (73 shorter events, 12.6 us)
Async XLA Ops:
  0.6 73.9 %copy-start = (bf16[1,256,2048]{2,1,0:T(8,128)(2,1)S(1)}, bf16[1,256,2048]{2,1,0:T(8,128)(2,1)}, u32[]{:S(2)}) copy-start(bf16[1,256,2048]{2,1,0:T(8,128)(2,1)} %param.39) | copy-start | bytes 3145732
  0.6 14.6 %copy-start.6 = (bf16[32,2048]{1,0:T(8,128)(2,1)S(1)}, bf16[32,2048]{1,0:T(8,128)(2,1)}, u32[]{:S(2)}) copy-start(bf16[32,2048]{1,0:T(8,128)(2,1)} %param.20) | copy-start | bytes 393220
  0.7 14.0 %copy-start.11 = (s32[32]{0:T(128)S(1)}, s32[32]{0:T(128)}, u32[]{:S(2)}) copy-start(s32[32]{0:T(128)} %param.30) | copy-start | bytes 388
  0.7 14.5 %copy-start.14 = (f32[2048]{0:T(1024)S(1)}, f32[2048]{0:T(1024)}, u32[]{:S(2)}) copy-start(f32[2048]{0:T(1024)} %param.21) | copy-start | bytes 24580
  0.7 14.0 %copy-start.4 = (f32[32,1,1024]{2,1,0:T(1,128)S(1)}, f32[32,1,1024]{2,1,0:T(1,128)}, u32[]{:S(2)}) copy-start(f32[32,1,1024]{2,1,0:T(1,128)} %param.29) | copy-start | bytes 393220
  0.7 14.5 %copy-start.12 = (bf16[2048,64]{0,1:T(8,128)(2,1)S(1)}, bf16[2048,64]{0,1:T(8,128)(2,1)}, u32[]{:S(2)}) copy-start(bf16[2048,64]{0,1:T(8,128)(2,1)} %param.23) | copy-start | bytes 786436
  5.0 11.8 %copy-start.1 = (bf16[32,1,1024,128]{3,2,1,0:T(8,128)(2,1)S(1)}, bf16[32,1,1024,128]{3,2,1,0:T(8,128)(2,1)}, u32[]{:S(2)}) copy-start(bf16[32,1,1024,128]{3,2,1,0:T(8,128)(2,1)} %param.28) | copy-start | bytes 25165828
  13.8 5.6 %copy-start.13 = (bf16[2048,64]{0,1:T(8,128)(2,1)S(1)}, bf16[2048,64]{0,1:T(8,128)(2,1)}, u32[]{:S(2)}) copy-start(bf16[2048,64]{0,1:T(8,128)(2,1)} %param.24) | copy-start | bytes 786436
  13.8 5.9 %copy-start.5 = (bf16[64,2048]{1,0:T(8,128)(2,1)S(1)}, bf16[64,2048]{1,0:T(8,128)(2,1)}, u32[]{:S(2)}) copy-start(bf16[64,2048]{1,0:T(8,128)(2,1)} %param.27) | copy-start | bytes 786436
  13.8 16.9 %copy-start.8 = (s32[32,6]{0,1:T(8,128)S(1)}, s32[32,6]{0,1:T(8,128)}, u32[]{:S(2)}) copy-start(s32[32,6]{0,1:T(8,128)} %param.32) | copy-start | bytes 2308
  13.8 18.6 %copy-start.10 = (f32[32,6]{0,1:T(8,128)S(1)}, f32[32,6]{0,1:T(8,128)}, u32[]{:S(2)}) copy-start(f32[32,6]{0,1:T(8,128)} %param.33) | copy-start | bytes 2308
  13.8 26.0 %copy-start.9 = (f32[2048]{0:T(1024)S(1)}, f32[2048]{0:T(1024)}, u32[]{:S(2)}) copy-start(f32[2048]{0:T(1024)} %param.31) | copy-start | bytes 24580
  15.2 58.7 %copy-start.2 = (bf16[1,2048,256]{2,1,0:T(8,128)(2,1)S(1)}, bf16[1,2048,256]{2,1,0:T(8,128)(2,1)}, u32[]{:S(2)}) copy-start(bf16[1,2048,256]{2,1,0:T(8,128)(2,1)} %param.37) | copy-start | bytes 3145732
  16.8 57.4 %copy-start.3 = (bf16[1,2048,256]{2,1,0:T(8,128)(2,1)S(1)}, bf16[1,2048,256]{2,1,0:T(8,128)(2,1)}, u32[]{:S(2)}) copy-start(bf16[1,2048,256]{2,1,0:T(8,128)(2,1)} %param.38) | copy-start | bytes 3145732
  20.7 18.9 %all-to-all-start = ((bf16[16,2,2048]{2,1,0:T(2,128)(2,1)}), bf16[16,2,2048]{2,1,0:T(2,128)(2,1)S(1)}, u32[]{:S(2)}, u32[]{:S(2)}) async-start(bf16[16,2,2048]{2,1,0:T(2,128)(2,1)} %reshape.219), calls=%async_computation | async-start | bytes 262144 | tf_op jit(solution)/shard_map/all_to_all | solution.py:16
  31.1 2.0 %copy-start.7 = (pred[32,16]{0,1:T(8,128)(4,1)}, pred[32,16]{0,1:T(8,128)(4,1)S(1)}, u32[]{:S(2)}) copy-start(pred[32,16]{0,1:T(8,128)(4,1)S(1)} %copy.40) | copy-start | bytes 1540
  59.2 13.7 %all-to-all-start.1 = ((bf16[16,2,2048]{2,1,0:T(2,128)(2,1)}), bf16[16,2,2048]{2,1,0:T(2,128)(2,1)}, u32[]{:S(2)}, u32[]{:S(2)}) async-start(bf16[16,2,2048]{2,1,0:T(2,128)(2,1)} %reshape.220), calls=%async_computation.1 | async-start | bytes 262144 | tf_op jit(solution)/shard_map/all_to_all | solution.py:143
  75.6 10.3 %all-to-all-start.2 = ((bf16[16,2,2048]{2,1,0:T(2,128)(2,1)}), bf16[16,2,2048]{2,1,0:T(2,128)(2,1)S(1)}, u32[]{:S(2)}, u32[]{:S(2)}) async-start(bf16[16,2,2048]{2,1,0:T(2,128)(2,1)} %copy.43), calls=%async_computation.2 | async-start | bytes 262144 | tf_op jit(solution)/shard_map/all_to_all | solution.py:153
  89.1 16.3 %all-to-all-start.3 = ((bf16[16,2,2048]{2,1,0:T(2,128)(2,1)}), bf16[16,2,2048]{2,1,0:T(2,128)(2,1)S(1)}, u32[]{:S(2)}, u32[]{:S(2)}) async-start(bf16[16,2,2048]{2,1,0:T(2,128)(2,1)} %reshape.222), calls=%async_computation.3 | async-start | bytes 262144 | tf_op jit(solution)/shard_map/all_to_all | solution.py:16
where the time goes:
time: 122 us; the launch traced here: 121 us
  blocking collectives  31.4 us (26%)
  starting transfers between devices  27.7 us (23%)
  waiting for transfers between devices  25.3 us (21%)
  matrix products  17.3 us (14%)
  other arithmetic  9.49 us (8%)
  local copies, waits for them, and re-layouts  8.9 us (7%)
    all_to_all x2, starting transfers between devices, summed_on_arrival(): lax.all_to_all(tiles, axis, split_axis=0, concat_axis=0, tiled=True)  17.4 us
    all_gather x1, blocking collectives, in_one_piece(): filled, at, outs = (lax.all_gather(both, axis, axis=dim, tiled=True), 0, [])  16.6 us
    all_gather x1, blocking collectives, body(): layer_out = lax.all_gather(out_slice, 'tp', axis=0, tiled=True)  14.8 us
    all_to_all x2, waiting for transfers between devices, summed_on_arrival(): lax.all_to_all(tiles, axis, split_axis=0, concat_axis=0, tiled=True)  14 us
    all_to_all x1, starting transfers between devices, body(): lax.all_to_all(dispatch, 'ep', split_axis=0, concat_axis=0, tiled=True)  6.8 us
    all_to_all x1, waiting for transfers between devices, body(): lax.all_to_all(served.astype(jnp.bfloat16), 'ep', split_axis=0, concat_ax...  5.74 us
    dot_general x1, matrix products, attend(): jnp.einsum('shd,shld->shl', queries, cached_keys, preferred_element_type=...  5.63 us
    all_to_all x1, waiting for transfers between devices, body(): lax.all_to_all(dispatch, 'ep', split_axis=0, concat_axis=0, tiled=True)  5.58 us
  transfers between devices with their start and end apart: 4, of which 4 were waited for; matrix products, arithmetic and copies ran while one was open for 5% of the time, Pallas kernels for 0%

commit v1 on v0

--- a/solution.py
+++ b/solution.py
@@ -165,7 +165,22 @@
     mixed_slice = summed_on_arrival((shared_part + routed).astype(jnp.bfloat16), "tp", 0)
     own_middle = lax.dynamic_slice_in_dim(middle, slice_start, slice_rows, 0)
     out_slice = (own_middle.astype(jnp.float32) + mixed_slice).astype(jnp.bfloat16)
-    layer_out = lax.all_gather(out_slice, "tp", axis=0, tiled=True)
+    all_rows, e_next, t1 = (lax.axis_size("tp"), lax.axis_index("tp"), out_slice.shape[0])
+    f_now, everything = (out_slice, 1)
+    while everything < all_rows:
+        f_now = jnp.concatenate(
+            [
+                f_now,
+                lax.ppermute(
+                    f_now,
+                    axis_name="tp",
+                    perm=[(k, (k - everything) % all_rows) for k in range(all_rows)],
+                ),
+            ],
+            axis=0,
+        )
+        everything = 2 * everything
+    layer_out = jnp.roll(f_now, e_next * t1, axis=0)
     return (layer_out, new_kv)
 
 

time: 122 us -> 125 us (1.025)
  blocking collectives: 31.4 us -> 16.6 us
  waiting for transfers between devices: 25.3 us -> 35.8 us
  starting transfers between devices: 27.7 us -> 33.8 us
    all_gather x1 -> x0, blocking collectives: 14.8 us -> none  [body(): layer_out = lax.all_gather(out_slice, 'tp', axis=0, tiled=True)]
    ppermute x0 -> x4, waiting for transfers between devices: none -> 9.18 us  [body(): lax.ppermute(f_now, axis_name='tp', perm=[(k, (k - everything) % all_rows...]
    ppermute x0 -> x4, starting transfers between devices: none -> 6.11 us  [body(): lax.ppermute(f_now, axis_name='tp', perm=[(k, (k - everything) % all_rows...]
    all_to_all x2, waiting for transfers between devices: 14 us -> 15.3 us  [summed_on_arrival(): lax.all_to_all(tiles, axis, split_axis=0, concat_axis=0, tiled=True)]
  transfers between devices with their start and end apart: 4 -> 8, of which waited for: 4 -> 8; matrix products, arithmetic and copies ran while one was open for 5% -> 5% of each run, Pallas kernels for 0% -> 0%
where the time goes in v1:
time: 125 us; the launch traced here: 123 us
  waiting for transfers between devices  35.8 us (29%)
  starting transfers between devices  33.8 us (27%)
  matrix products  17.3 us (14%)
  blocking collectives  16.6 us (13%)
  other arithmetic  9.6 us (8%)
  local copies, waits for them, and re-layouts  8.99 us (7%)
    all_to_all x2, starting transfers between devices, summed_on_arrival(): lax.all_to_all(tiles, axis, split_axis=0, concat_axis=0, tiled=True)  17.4 us
    all_gather x1, blocking collectives, in_one_piece(): filled, at, outs = (lax.all_gather(both, axis, axis=dim, tiled=True), 0, [])  16.6 us
    all_to_all x2, waiting for transfers between devices, summed_on_arrival(): lax.all_to_all(tiles, axis, split_axis=0, concat_axis=0, tiled=True)  15.3 us
    ppermute x4, waiting for transfers between devices, body(): lax.ppermute(f_now, axis_name='tp', perm=[(k, (k - everything) % all_rows...  9.18 us
    all_to_all x1, starting transfers between devices, body(): lax.all_to_all(dispatch, 'ep', split_axis=0, concat_axis=0, tiled=True)  6.8 us
    ppermute x4, starting transfers between devices, body(): lax.ppermute(f_now, axis_name='tp', perm=[(k, (k - everything) % all_rows...  6.11 us
    all_to_all x1, waiting for transfers between devices, body(): lax.all_to_all(served.astype(jnp.bfloat16), 'ep', split_axis=0, concat_ax...  5.75 us
    dot_general x1, matrix products, attend(): jnp.einsum('shd,shld->shl', queries, cached_keys, preferred_element_type=...  5.63 us
  transfers between devices with their start and end apart: 8, of which 8 were waited for; matrix products, arithmetic and copies ran while one was open for 5% of the time, Pallas kernels for 0%

profile of v1, /device:TPU:1, one launch (start us, length us, event | category | flops | bytes accessed | tf_op | source)
XLA Modules:
  0.0 123.1 jit_solution(7583507851891789798)
XLA Ops:
  0.7 1.1 fusion.13
  3.7 1.3 %convolution_convert_fusion.5 = bf16[32,64]{1,0:T(8,128)(2,1)S(1)} fusion(bf16[2048,64]{0,1:T(8,128)(2,1)} %param.22, bf16[32,2048]{1,0:T(8,128)(2,1)} %param.20, f32[2048]{0:T(1024)} %param.21, f32[32]{0:T(128)S(1)} %add_rsqrt_fusion.1), kind=kOutput, calls=%fused_computation.18 | convolution fusion | flops 8652800 | bytes 405632 | tf_op jit(solution)/shard_map/dot_general | solution.py:36
  5.0 1.4 %dynamic-slice = f32[1]{0:T(128)} dynamic-slice(f32[16]{0:T(128)} %param.26, s32[]{:T(128)S(6)} %select_n.42), dynamic_slice_sizes={1} | dynamic-slice | bytes 12 | tf_op jit(solution)/shard_map/dynamic_slice | solution.py:101
  6.4 1.8 %fusion.21 = f32[32]{0:T(128)S(1)} fusion(f32[32,1,1024]{2,1,0:T(1,128)} %param.29, s32[32]{0:T(128)S(1)} %broadcast_add_fusion), kind=kLoop, calls=%fused_computation.39 | loop fusion | flops 98272 | bytes 131328 | tf_op jit(solution)/shard_map/reduce_sum | solution.py:45
  8.1 5.6 %fusion.2 = f32[32,1,1024]{2,1,0:T(1,128)S(1)} fusion(bf16[32,1,1024,128]{3,2,1,0:T(8,128)(2,1)} %param.28, bf16[32,64,1]{1,0,2:T(8,128)(2,1)S(1)} %bitcast.52), kind=kOutput, calls=%fused_computation.2 | convolution fusion | flops 4194304 | bytes 8523776 | tf_op jit(solution)/shard_map/shd,shld->shl/dot_general | solution.py:50
  16.8 2.6 %fusion = f32[32,1,64]{2,1,0:T(1,128)S(1)} fusion(bf16[32,1,1024,128]{3,2,1,0:T(8,128)(2,1)S(1)} %copy-done.1, f32[32]{0:T(128)S(1)} %get-tuple-element.9, f32[32,1,1024]{2,1,0:T(1,128)S(1)} %get-tuple-element.5, f32[32]{0:T(128)S(1)} %multiply_maximum_fusion), kind=kOutput, calls=%fused_computation | convolution fusion | flops 4292608 | bytes 8528128 | tf_op jit(solution)/shard_map/shl,shld->shd/dot_general | solution.py:61
  20.7 10.0 %all-to-all-start = ((bf16[16,2,2048]{2,1,0:T(2,128)(2,1)}), bf16[16,2,2048]{2,1,0:T(2,128)(2,1)S(1)}, u32[]{:S(2)}, u32[]{:S(2)}) async-start(bf16[16,2,2048]{2,1,0:T(2,128)(2,1)} %reshape.219), calls=%async_computation | async-start | bytes 262144 | tf_op jit(solution)/shard_map/all_to_all | solution.py:16
  33.1 6.5 %all-to-all-done = bf16[16,2,2048]{2,1,0:T(2,128)(2,1)S(1)} async-done(((bf16[16,2,2048]{2,1,0:T(2,128)(2,1)}), bf16[16,2,2048]{2,1,0:T(2,128)(2,1)S(1)}, u32[]{:S(2)}, u32[]{:S(2)}) %all-to-all-start) | async-done | bytes 131104 | tf_op jit(solution)/shard_map/all_to_all | solution.py:16
  39.9 16.6 %all-gather = bf16[16,2,4096]{2,1,0:T(2,128)(2,1)} all-gather(bf16[1,2,4096]{2,1,0:T(2,128)(2,1)S(1)} %maximum_bitcast_fusion), channel_id=1, replica_groups=mesh['ep'=16,'tp'=16] {'tp'}, dimensions={0}, use_global_device_ids=true | all-gather | bytes 278528 | tf_op jit(solution)/shard_map/all_gather | solution.py:22
  59.2 6.8 %all-to-all-start.1 = ((bf16[16,2,2048]{2,1,0:T(2,128)(2,1)}), bf16[16,2,2048]{2,1,0:T(2,128)(2,1)}, u32[]{:S(2)}, u32[]{:S(2)}) async-start(bf16[16,2,2048]{2,1,0:T(2,128)(2,1)} %reshape.220), calls=%async_computation.1 | async-start | bytes 262144 | tf_op jit(solution)/shard_map/all_to_all | solution.py:143
  66.0 1.3 %and_select_fusion = f32[32,16,2]{0,2,1:T(2,128)} fusion(pred[32,16]{0,1:T(8,128)(4,1)} %copy-done.7, f32[32,16]{0,1:T(8,128)} %fusion.28, s32[32,16]{0,1:T(8,128)S(1)} %copy.41), kind=kLoop, calls=%fused_computation.50 | loop fusion | flops 3072 | bytes 8704 | tf_op jit(solution)/shard_map/mul | solution.py:156
  67.4 5.6 %all-to-all-done.1 = bf16[16,2,2048]{2,1,0:T(2,128)(2,1)} async-done(((bf16[16,2,2048]{2,1,0:T(2,128)(2,1)}), bf16[16,2,2048]{2,1,0:T(2,128)(2,1)}, u32[]{:S(2)}, u32[]{:S(2)}) %all-to-all-start.1) | async-done | bytes 131104 | tf_op jit(solution)/shard_map/all_to_all | solution.py:143
  75.6 3.5 %all-to-all-start.2 = ((bf16[16,2,2048]{2,1,0:T(2,128)(2,1)}), bf16[16,2,2048]{2,1,0:T(2,128)(2,1)S(1)}, u32[]{:S(2)}, u32[]{:S(2)}) async-start(bf16[16,2,2048]{2,1,0:T(2,128)(2,1)} %copy.43), calls=%async_computation.2 | async-start | bytes 262144 | tf_op jit(solution)/shard_map/all_to_all | solution.py:153
  80.2 5.7 %all-to-all-done.2 = bf16[16,2,2048]{2,1,0:T(2,128)(2,1)S(1)} async-done(((bf16[16,2,2048]{2,1,0:T(2,128)(2,1)}), bf16[16,2,2048]{2,1,0:T(2,128)(2,1)S(1)}, u32[]{:S(2)}, u32[]{:S(2)}) %all-to-all-start.2) | async-done | bytes 131104 | tf_op jit(solution)/shard_map/all_to_all | solution.py:153
  87.0 1.3 %fusion.6 = bf16[32,2048]{1,0:T(8,128)(2,1)S(1)} fusion(f32[32,2048]{1,0:T(8,128)S(1)} %convolution_bitcast_fusion, bf16[32,2048]{1,0:T(8,128)(2,1)} %param.36, bf16[2048,32]{0,1:T(8,128)(2,1)} %param.35, bf16[32,4096]{1,0:T(8,128)(2,1)S(1)} %reshape.226, f32[32,32]{1,0:T(8,128)S(1)} %fusion.25), kind=kOutput, calls=%fused_computation.8 | convolution fusion | flops 8525824 | bytes 802816 | tf_op jit(solution)/shard_map/dot_general | solution.py:119
  89.1 7.4 %all-to-all-start.3 = ((bf16[16,2,2048]{2,1,0:T(2,128)(2,1)}), bf16[16,2,2048]{2,1,0:T(2,128)(2,1)S(1)}, u32[]{:S(2)}, u32[]{:S(2)}) async-start(bf16[16,2,2048]{2,1,0:T(2,128)(2,1)} %reshape.222), calls=%async_computation.3 | async-start | bytes 262144 | tf_op jit(solution)/shard_map/all_to_all | solution.py:16
  96.5 8.9 %all-to-all-done.3 = bf16[16,2,2048]{2,1,0:T(2,128)(2,1)S(1)} async-done(((bf16[16,2,2048]{2,1,0:T(2,128)(2,1)}), bf16[16,2,2048]{2,1,0:T(2,128)(2,1)S(1)}, u32[]{:S(2)}, u32[]{:S(2)}) %all-to-all-start.3) | async-done | bytes 131104 | tf_op jit(solution)/shard_map/all_to_all | solution.py:16
  105.5 3.1 %collective-permute-done = bf16[2,2048]{1,0:T(2,128)(2,1)S(1)} collective-permute-done((bf16[2,2048]{1,0:T(2,128)(2,1)S(1)}, bf16[2,2048]{1,0:T(2,128)(2,1)S(1)}, u32[]{:S(2)}, u32[]{:S(2)}) %collective-permute-start) | collective-permute-done | bytes 8224 | tf_op jit(solution)/shard_map/ppermute | solution.py:174
  108.6 1.3 %collective-permute-start.1 = (bf16[4,2048]{1,0:T(4,128)(2,1)S(1)}, bf16[4,2048]{1,0:T(4,128)(2,1)S(1)}, u32[]{:S(2)}, u32[]{:S(2)}) collective-permute-start(bf16[4,2048]{1,0:T(4,128)(2,1)S(1)} %pad_maximum_fusion.2), channel_id=1, source_target_pairs={{0,14},{1,15},{2,0},{3,1},{4,2},{5,3},{6,4},{7,5},{8,6},{9,7},{10,... | collective-permute-start | bytes 49160 | tf_op jit(solution)/shard_map/ppermute | solution.py:174
  110.0 1.3 %collective-permute-done.1 = bf16[4,2048]{1,0:T(4,128)(2,1)S(1)} collective-permute-done((bf16[4,2048]{1,0:T(4,128)(2,1)S(1)}, bf16[4,2048]{1,0:T(4,128)(2,1)S(1)}, u32[]{:S(2)}, u32[]{:S(2)}) %collective-permute-start.1) | collective-permute-done | bytes 16416 | tf_op jit(solution)/shard_map/ppermute | solution.py:174
  112.4 2.7 %collective-permute-done.2 = bf16[8,2048]{1,0:T(8,128)(2,1)S(1)} collective-permute-done((bf16[8,2048]{1,0:T(8,128)(2,1)S(1)}, bf16[8,2048]{1,0:T(8,128)(2,1)S(1)}, u32[]{:S(2)}, u32[]{:S(2)}) %collective-permute-start.2) | collective-permute-done | bytes 32800 | tf_op jit(solution)/shard_map/ppermute | solution.py:174
  115.1 3.7 %collective-permute-start.3 = (bf16[16,2048]{1,0:T(8,128)(2,1)S(1)}, bf16[16,2048]{1,0:T(8,128)(2,1)S(1)}, u32[]{:S(2)}, u32[]{:S(2)}) collective-permute-start(bf16[16,2048]{1,0:T(8,128)(2,1)S(1)} %pad_maximum_fusion), channel_id=1, source_target_pairs={{0,8},{1,9},{2,10},{3,11},{4,12},{5,13},{6,14},{7,15},{8,0},{9,1},... | collective-permute-start | bytes 196616 | tf_op jit(solution)/shard_map/ppermute | solution.py:174
  118.8 1.4 %pad_maximum_fusion.3 = bf16[32,1,128]{2,0,1:T(8,128)(2,1)} fusion(bf16[32,1,64]{2,0,1:T(8,128)(2,1)S(1)} %bitcast.53, bf16[32,1,64]{2,0,1:T(8,128)(2,1)} %bitcast.55), kind=kLoop, calls=%fused_computation.74 | loop fusion | flops 16384 | bytes 16384 | tf_op jit(solution)/shard_map/concatenate | solution.py:98
  120.2 2.1 %collective-permute-done.3 = bf16[16,2048]{1,0:T(8,128)(2,1)S(1)} collective-permute-done((bf16[16,2048]{1,0:T(8,128)(2,1)S(1)}, bf16[16,2048]{1,0:T(8,128)(2,1)S(1)}, u32[]{:S(2)}, u32[]{:S(2)}) %collective-permute-start.3) | collective-permute-done | bytes 65568 | tf_op jit(solution)/shard_map/ppermute | solution.py:174
  (84 shorter events, 19.2 us)
Async XLA Ops:
  0.6 73.9 %copy-start = (bf16[1,256,2048]{2,1,0:T(8,128)(2,1)S(1)}, bf16[1,256,2048]{2,1,0:T(8,128)(2,1)}, u32[]{:S(2)}) copy-start(bf16[1,256,2048]{2,1,0:T(8,128)(2,1)} %param.39) | copy-start | bytes 3145732
  0.6 14.6 %copy-start.6 = (bf16[32,2048]{1,0:T(8,128)(2,1)S(1)}, bf16[32,2048]{1,0:T(8,128)(2,1)}, u32[]{:S(2)}) copy-start(bf16[32,2048]{1,0:T(8,128)(2,1)} %param.20) | copy-start | bytes 393220
  0.7 14.0 %copy-start.11 = (s32[32]{0:T(128)S(1)}, s32[32]{0:T(128)}, u32[]{:S(2)}) copy-start(s32[32]{0:T(128)} %param.30) | copy-start | bytes 388
  0.7 14.5 %copy-start.14 = (f32[2048]{0:T(1024)S(1)}, f32[2048]{0:T(1024)}, u32[]{:S(2)}) copy-start(f32[2048]{0:T(1024)} %param.21) | copy-start | bytes 24580
  0.7 14.0 %copy-start.4 = (f32[32,1,1024]{2,1,0:T(1,128)S(1)}, f32[32,1,1024]{2,1,0:T(1,128)}, u32[]{:S(2)}) copy-start(f32[32,1,1024]{2,1,0:T(1,128)} %param.29) | copy-start | bytes 393220
  0.7 14.5 %copy-start.12 = (bf16[2048,64]{0,1:T(8,128)(2,1)S(1)}, bf16[2048,64]{0,1:T(8,128)(2,1)}, u32[]{:S(2)}) copy-start(bf16[2048,64]{0,1:T(8,128)(2,1)} %param.23) | copy-start | bytes 786436
  5.0 11.8 %copy-start.1 = (bf16[32,1,1024,128]{3,2,1,0:T(8,128)(2,1)S(1)}, bf16[32,1,1024,128]{3,2,1,0:T(8,128)(2,1)}, u32[]{:S(2)}) copy-start(bf16[32,1,1024,128]{3,2,1,0:T(8,128)(2,1)} %param.28) | copy-start | bytes 25165828
  13.8 5.6 %copy-start.13 = (bf16[2048,64]{0,1:T(8,128)(2,1)S(1)}, bf16[2048,64]{0,1:T(8,128)(2,1)}, u32[]{:S(2)}) copy-start(bf16[2048,64]{0,1:T(8,128)(2,1)} %param.24) | copy-start | bytes 786436
  13.8 5.9 %copy-start.5 = (bf16[64,2048]{1,0:T(8,128)(2,1)S(1)}, bf16[64,2048]{1,0:T(8,128)(2,1)}, u32[]{:S(2)}) copy-start(bf16[64,2048]{1,0:T(8,128)(2,1)} %param.27) | copy-start | bytes 786436
  13.8 16.9 %copy-start.8 = (s32[32,6]{0,1:T(8,128)S(1)}, s32[32,6]{0,1:T(8,128)}, u32[]{:S(2)}) copy-start(s32[32,6]{0,1:T(8,128)} %param.32) | copy-start | bytes 2308
  13.8 18.6 %copy-start.10 = (f32[32,6]{0,1:T(8,128)S(1)}, f32[32,6]{0,1:T(8,128)}, u32[]{:S(2)}) copy-start(f32[32,6]{0,1:T(8,128)} %param.33) | copy-start | bytes 2308
  13.8 26.0 %copy-start.9 = (f32[2048]{0:T(1024)S(1)}, f32[2048]{0:T(1024)}, u32[]{:S(2)}) copy-start(f32[2048]{0:T(1024)} %param.31) | copy-start | bytes 24580
  15.2 58.7 %copy-start.2 = (bf16[1,2048,256]{2,1,0:T(8,128)(2,1)S(1)}, bf16[1,2048,256]{2,1,0:T(8,128)(2,1)}, u32[]{:S(2)}) copy-start(bf16[1,2048,256]{2,1,0:T(8,128)(2,1)} %param.37) | copy-start | bytes 3145732
  16.8 57.4 %copy-start.3 = (bf16[1,2048,256]{2,1,0:T(8,128)(2,1)S(1)}, bf16[1,2048,256]{2,1,0:T(8,128)(2,1)}, u32[]{:S(2)}) copy-start(bf16[1,2048,256]{2,1,0:T(8,128)(2,1)} %param.38) | copy-start | bytes 3145732
  20.7 18.9 %all-to-all-start = ((bf16[16,2,2048]{2,1,0:T(2,128)(2,1)}), bf16[16,2,2048]{2,1,0:T(2,128)(2,1)S(1)}, u32[]{:S(2)}, u32[]{:S(2)}) async-start(bf16[16,2,2048]{2,1,0:T(2,128)(2,1)} %reshape.219), calls=%async_computation | async-start | bytes 262144 | tf_op jit(solution)/shard_map/all_to_all | solution.py:16
  31.1 2.0 %copy-start.7 = (pred[32,16]{0,1:T(8,128)(4,1)}, pred[32,16]{0,1:T(8,128)(4,1)S(1)}, u32[]{:S(2)}) copy-start(pred[32,16]{0,1:T(8,128)(4,1)S(1)} %copy.40) | copy-start | bytes 1540
  59.2 13.7 %all-to-all-start.1 = ((bf16[16,2,2048]{2,1,0:T(2,128)(2,1)}), bf16[16,2,2048]{2,1,0:T(2,128)(2,1)}, u32[]{:S(2)}, u32[]{:S(2)}) async-start(bf16[16,2,2048]{2,1,0:T(2,128)(2,1)} %reshape.220), calls=%async_computation.1 | async-start | bytes 262144 | tf_op jit(solution)/shard_map/all_to_all | solution.py:143
  75.6 10.3 %all-to-all-start.2 = ((bf16[16,2,2048]{2,1,0:T(2,128)(2,1)}), bf16[16,2,2048]{2,1,0:T(2,128)(2,1)S(1)}, u32[]{:S(2)}, u32[]{:S(2)}) async-start(bf16[16,2,2048]{2,1,0:T(2,128)(2,1)} %copy.43), calls=%async_computation.2 | async-start | bytes 262144 | tf_op jit(solution)/shard_map/all_to_all | solution.py:153
  89.1 16.3 %all-to-all-start.3 = ((bf16[16,2,2048]{2,1,0:T(2,128)(2,1)}), bf16[16,2,2048]{2,1,0:T(2,128)(2,1)S(1)}, u32[]{:S(2)}, u32[]{:S(2)}) async-start(bf16[16,2,2048]{2,1,0:T(2,128)(2,1)} %reshape.222), calls=%async_computation.3 | async-start | bytes 262144 | tf_op jit(solution)/shard_map/all_to_all | solution.py:16
  105.5 3.1 %collective-permute-start = (bf16[2,2048]{1,0:T(2,128)(2,1)S(1)}, bf16[2,2048]{1,0:T(2,128)(2,1)S(1)}, u32[]{:S(2)}, u32[]{:S(2)}) collective-permute-start(bf16[2,2048]{1,0:T(2,128)(2,1)S(1)} %add_convert_fusion), channel_id=1, source_target_pairs={{0,15},{1,0},{2,1},{3,2},{4,3},{5,4},{6,5},{7,6},{8,7},{9,8},{10,9... | collective-permute-start | bytes 24584 | tf_op jit(solution)/shard_map/ppermute | solution.py:174
  108.6 2.7 %collective-permute-start.1 = (bf16[4,2048]{1,0:T(4,128)(2,1)S(1)}, bf16[4,2048]{1,0:T(4,128)(2,1)S(1)}, u32[]{:S(2)}, u32[]{:S(2)}) collective-permute-start(bf16[4,2048]{1,0:T(4,128)(2,1)S(1)} %pad_maximum_fusion.2), channel_id=1, source_target_pairs={{0,14},{1,15},{2,0},{3,1},{4,2},{5,3},{6,4},{7,5},{8,6},{9,7},{10,... | collective-permute-start | bytes 49160 | tf_op jit(solution)/shard_map/ppermute | solution.py:174
  111.3 3.7 %collective-permute-start.2 = (bf16[8,2048]{1,0:T(8,128)(2,1)S(1)}, bf16[8,2048]{1,0:T(8,128)(2,1)S(1)}, u32[]{:S(2)}, u32[]{:S(2)}) collective-permute-start(bf16[8,2048]{1,0:T(8,128)(2,1)S(1)} %pad_maximum_fusion.1), channel_id=1, source_target_pairs={{0,12},{1,13},{2,14},{3,15},{4,0},{5,1},{6,2},{7,3},{8,4},{9,5},{1... | collective-permute-start | bytes 98312 | tf_op jit(solution)/shard_map/ppermute | solution.py:174
  115.1 7.2 %collective-permute-start.3 = (bf16[16,2048]{1,0:T(8,128)(2,1)S(1)}, bf16[16,2048]{1,0:T(8,128)(2,1)S(1)}, u32[]{:S(2)}, u32[]{:S(2)}) collective-permute-start(bf16[16,2048]{1,0:T(8,128)(2,1)S(1)} %pad_maximum_fusion), channel_id=1, source_target_pairs={{0,8},{1,9},{2,10},{3,11},{4,12},{5,13},{6,14},{7,15},{8,0},{9,1},... | collective-permute-start | bytes 196616 | tf_op jit(solution)/shard_map/ppermute | solution.py:174
